TPU v7x, 768 devices: a whole 4x8x12 slice. The times are simulated.
768 devices in a mesh: ep: 24 (over z, core), tp: 32 (over y, x).
Axes of the slice: x: 4, y: 8, z: 12, core: 2. Of those that a mesh axis runs over, the one named last changes fastest.
Arguments:
- tokens: bfloat16 [3072, 2048], P('ep', 'tp'), may hold values from -6 to 6
- out_grad: bfloat16 [3072, 2048], P('ep', 'tp'), may hold values from -6 to 6
- routes: int32 [3072, 2], P('ep'), may hold values from 0 to 23, all different within a row; in each aligned block of 128 rows (0 to 127, 128 to 255, ...) at most 16 rows name the same one
- gates: float32 [3072, 2], P('ep'), may hold values from 0.1 to 0.9
- gate_weight: bfloat16 [24, 2048, 5632], P('ep', None, 'tp'), may hold values from -0.125 to 0.125
- up_weight: bfloat16 [24, 2048, 5632], P('ep', None, 'tp'), may hold values from -0.125 to 0.125
- down_weight: bfloat16 [24, 5632, 2048], P('ep', 'tp'), may hold values from -0.078125 to 0.078125
Outputs:
- tokens_grad: bfloat16 [3072, 2048], P('ep', 'tp')
- gates_grad: float32 [3072, 2], P(('ep', 'tp'))
- gate_weight_grad: bfloat16 [24, 2048, 5632], P('ep', None, 'tp')
- up_weight_grad: bfloat16 [24, 2048, 5632], P('ep', None, 'tp')
- down_weight_grad: bfloat16 [24, 5632, 2048], P('ep', 'tp')
Inputs may be any that keep to these rules, and one draw needn't show every extreme that they name: `routes`: the 2 experts of a token differ. In each aligned block of 128 rows (the tokens of one index of ep) no expert is named by more than 16 rows, a bound that some block reaches.
All inputs are finite; a program needn't handle non-finite values.
Results may differ from a plain program's by a relative error of at most 0.029.
Values may be sent and summed in bfloat16 or wider, within the bound.
No kernel may reach another device: no remote copies, remote signals or barrier semaphores. Data moves between devices by JAX's collectives and lax.ppermute only.
A program may use at most 64 MiB of HBM per device.

v0:
```python
import functools

import jax
import jax.numpy as jnp
from jax import lax
from jax.experimental import pallas as pl
from jax.experimental.pallas import tpu as pltpu
from jax.sharding import Mesh
from jax.sharding import PartitionSpec as P

TP = ("yh", "yl", "x")
NEAR = ("yl", "x")
BF16 = jnp.bfloat16
F32 = jnp.float32
I32 = jnp.int32
CPU_INTERPRET = False


def call(body, outs, flops=0, n_scalars=0, limit=12):
    def run(*args):
        smem = pl.BlockSpec(memory_space=pltpu.SMEM)
        vmem = pl.BlockSpec(memory_space=pltpu.VMEM)
        size = sum(a.size * a.dtype.itemsize for a in args)
        return pl.pallas_call(
            body,
            out_shape=[jax.ShapeDtypeStruct(s, d) for s, d in outs],
            in_specs=[smem if k < n_scalars else vmem for k in range(len(args))],
            out_specs=[vmem] * len(outs),
            compiler_params=pltpu.CompilerParams(vmem_limit_bytes=limit * 2**20),
            cost_estimate=pl.CostEstimate(flops=flops, transcendentals=0, bytes_accessed=size),
            interpret=CPU_INTERPRET,
        )(*args)

    return run


def dot(a, b, dims):
    return lax.dot_general(a, b, (dims, ((), ())), preferred_element_type=F32)


def iota(shape, dim):
    return lax.broadcasted_iota(I32, shape, dim)


def dot_rows(dots):
    high = dots.astype(BF16).astype(F32)
    row = iota((8, dots.shape[1]), 0)
    return jnp.where(row == 0, high, jnp.where(row == 1, dots - high, 0.0))


def place_body(table_ref, sent_ref, dest_ref, *, n_ep, cap, top_k):
    toks = table_ref.shape[1]
    both = table_ref.shape[0] - 2 * top_k
    feats = both // 2
    routes = table_ref[both : both + top_k].astype(I32)
    gates = table_ref[both + top_k :]
    experts = -(-n_ep // 16) * 16
    hot = [(iota((experts, toks), 0) == routes[k : k + 1]).astype(BF16) for k in range(top_k)]
    hot = jnp.concatenate(hot, axis=1)
    slots = top_k * toks
    earlier = (iota((slots, slots), 0) < iota((slots, slots), 1)).astype(BF16)
    rank = jnp.sum(dot(hot, earlier, ((1,), (0,))) * hot.astype(F32), axis=0, keepdims=True)
    rank = rank.astype(I32)
    rows = n_ep * cap
    place = iota((rows, toks), 0)
    select = jnp.zeros((rows, toks), F32)
    weight = jnp.zeros((rows, 1), F32)
    for k in range(top_k):
        dest = routes[k : k + 1] * cap + rank[:, k * toks : (k + 1) * toks]
        dest_ref[k : k + 1, :] = dest
        at = place == dest
        select = select + jnp.where(at, 1.0, 0.0)
        weight = weight + jnp.sum(jnp.where(at, gates[k : k + 1], 0.0), axis=1, keepdims=True)
    moved = dot(select.astype(BF16), table_ref[:both].astype(BF16), ((1,), (1,)))
    lane = iota(moved.shape, 1)
    sent_ref[...] = jnp.where(lane < feats, moved, moved * weight).astype(BF16)


def turn_body(got_ref, out_ref):
    turned = got_ref[...].astype(F32).T.astype(BF16)
    for k in range(out_ref.shape[0]):
        out_ref[k] = turned


def column(rows_ref, yh, yl, part):
    _, _, both, _ = rows_ref.shape
    feats = both // 2
    n_x = rows_ref.shape[0] // 2
    at = slice(part * feats, (part + 1) * feats)
    return jnp.concatenate([rows_ref[yl * n_x + x, yh, at] for x in range(n_x)], axis=0)


def expert_body(rows_ref, wg_ref, wu_ref, wd_ref, out_ref, parts_ref):
    n_near, n_yh, both, _ = rows_ref.shape
    feats = both // 2
    n_x = n_near // 2
    hid = wg_ref.shape[0]
    order = [(yh, yl) for yh in range(n_yh) for yl in range(2)]
    x_t = jnp.concatenate([column(rows_ref, yh, yl, 0) for yh, yl in order], axis=0)
    pre_gate = jnp.dot(wg_ref[...], x_t, preferred_element_type=F32)
    pre_up = jnp.dot(wu_ref[...], x_t, preferred_element_type=F32)
    c_t = jnp.concatenate([column(rows_ref, yh, yl, 1) for yh, yl in order], axis=0)
    hid_grad = jnp.dot(wd_ref[...], c_t, preferred_element_type=F32)
    sig = jax.nn.sigmoid(pre_gate)
    act = pre_gate * sig
    hidden = (act * pre_up).astype(BF16)
    gate_part = (hid_grad * pre_up * sig * (1.0 + pre_gate * (1.0 - sig))).astype(BF16)
    up_part = (hid_grad * act).astype(BF16)
    dots = jnp.sum(hidden.astype(F32) * hid_grad, axis=0, keepdims=True)
    parts_ref[0:hid] = gate_part
    parts_ref[hid : 2 * hid] = up_part
    parts_ref[2 * hid : 3 * hid] = hidden
    parts = parts_ref[0 : 2 * hid]
    tail = dot_rows(dots).astype(BF16)
    for k, (yh, yl) in enumerate(order):
        cols = slice(k * n_x * feats, (k + 1) * n_x * feats)
        w = jnp.concatenate([wg_ref[:, cols], wu_ref[:, cols]], axis=0)
        piece = dot(w, parts, ((0,), (0,))).astype(BF16)
        for x in range(n_x):
            at = slice(yh * feats, (yh + 1) * feats)
            out_ref[yl * n_x + x, at] = piece[x * feats : (x + 1) * feats]
    for k in range(n_near):
        out_ref[k, n_yh * feats :] = tail


def weights_body(parts_ref, rows_ref, gate_ref, up_ref, down_ref):
    n_near, n_yh, both, _ = rows_ref.shape
    wide = n_near // 2 * (both // 2)
    hid = gate_ref.shape[0]
    for yh in range(n_yh):
        for yl in range(2):
            k = 2 * yh + yl
            cols = slice(k * wide, (k + 1) * wide)
            x_t, c_t = column(rows_ref, yh, yl, 0), column(rows_ref, yh, yl, 1)
            grads = dot(parts_ref[0 : 2 * hid], x_t, ((1,), (1,))).astype(BF16)
            gate_ref[:, cols] = grads[:hid]
            up_ref[:, cols] = grads[hid:]
            down_ref[:, cols] = dot(parts_ref[2 * hid :], c_t, ((1,), (1,))).astype(BF16)


def near_body(in_ref, out_ref):
    n, height, _ = in_ref.shape
    n_y, tall, _ = out_ref.shape
    feats = tall - 8
    for y in range(n_y):
        total = in_ref[0, y * feats : (y + 1) * feats].astype(F32)
        for k in range(1, n):
            total = total + in_ref[k, y * feats : (y + 1) * feats].astype(F32)
        out_ref[y, :feats] = total.astype(BF16)
    tail = in_ref[0, height - 8 :].astype(F32)
    for k in range(1, n):
        tail = tail + in_ref[k, height - 8 :].astype(F32)
    tail = dot_rows(jnp.sum(tail, axis=0, keepdims=True)).astype(BF16)
    for y in range(n_y):
        out_ref[y, feats:] = tail


def far_body(in_ref, out_ref):
    n, tall, rows = in_ref.shape
    total = in_ref[0].astype(F32)
    for k in range(1, n):
        total = total + in_ref[k].astype(F32)
    feats = tall - 8
    tail = dot_rows(jnp.sum(total[feats:], axis=0, keepdims=True))
    rest = jnp.zeros((out_ref.shape[1] - tall, rows), F32)
    whole = jnp.concatenate([total[:feats], tail, rest], axis=0)
    out_ref[...] = whole.T.astype(BF16)


def final_body(start_ref, back_ref, dest_ref, gates_ref, tokens_ref, ratio_ref):
    rows, lanes = back_ref.shape
    feats, toks = tokens_ref.shape
    top_k, share = ratio_ref.shape
    back = back_ref[...]
    dots = back[:, feats : feats + 1].astype(F32) + back[:, feats + 1 : feats + 2].astype(F32)
    place = iota((rows, toks), 0)
    select = jnp.zeros((rows, toks), F32)
    start = start_ref[0]
    for k in range(top_k):
        at = place == dest_ref[k : k + 1, :]
        select = select + jnp.where(at, 1.0, 0.0)
        mine = jnp.sum(jnp.where(at, dots, 0.0), axis=0, keepdims=True) / gates_ref[k : k + 1, :]
        for j in range(share):
            here = iota((1, toks), 1) == start + j
            ratio_ref[k : k + 1, j : j + 1] = jnp.sum(jnp.where(here, mine, 0.0), axis=1, keepdims=True)
    summed = dot(back, select.astype(BF16), ((0,), (0,)))
    tokens_ref[...] = summed[:feats].astype(BF16)


def exchange(array, axis):
    return lax.all_to_all(array, axis, split_axis=0, concat_axis=0, tiled=True)


def on_device(tokens, out_grad, routes, gates, gate_weight, up_weight, down_weight):
    tok_dev, top_k = routes.shape
    n_ep, n_yh, n_near = lax.axis_size("ep"), lax.axis_size("yh"), lax.axis_size(NEAR)
    cap = (3 * tok_dev + n_ep - 1) // n_ep
    rows = n_ep * cap
    feats = tokens.shape[1]
    both = 2 * feats
    w_gate, w_up, w_down = gate_weight[0].T, up_weight[0].T, down_weight[0]
    hid, width = w_gate.shape

    table = jnp.concatenate(
        [a.T.astype(F32) for a in (tokens, out_grad, routes, gates)], axis=0
    )
    sent, dest = call(
        functools.partial(place_body, n_ep=n_ep, cap=cap, top_k=top_k),
        [((rows, both), BF16), ((top_k, tok_dev), I32)],
    )(table)
    got = exchange(sent.reshape(n_ep, cap, both), "ep").reshape(rows, both)
    (copies,) = call(turn_body, [((n_yh, both, rows), BF16)])(got)
    some = exchange(copies, "yh")
    every = exchange(jnp.broadcast_to(some[None], (n_near, *some.shape)), NEAR)

    chunks, parts = call(
        expert_body,
        [((n_near, n_yh * feats + 8, rows), BF16), ((3 * hid, rows), BF16)],
        flops=10 * hid * width * rows,
        limit=20,
    )(every, w_gate, w_up, w_down)
    swapped = exchange(chunks, NEAR)
    gate_grad, up_grad, down_grad = call(
        weights_body, [((hid, width), BF16)] * 3, flops=6 * hid * width * rows, limit=20
    )(parts, every)
    (near,) = call(near_body, [((n_yh, feats + 8, rows), BF16)])(swapped)
    (packed,) = call(far_body, [((rows, both), BF16)])(exchange(near, "yh"))
    back = exchange(packed.reshape(n_ep, cap, both), "ep").reshape(rows, both)
    share = tok_dev // (n_yh * n_near)
    start = (lax.axis_index(TP).astype(I32) * share).reshape(1)
    tokens_grad, ratio = call(
        final_body, [((feats, tok_dev), BF16), ((top_k, share), F32)], n_scalars=1
    )(start, back, dest, gates.T)
    return (
        tokens_grad.T,
        ratio.T,
        gate_grad.T[None],
        up_grad.T[None],
        down_grad[None],
    )


def solution(mesh):
    torus = Mesh(mesh.devices.reshape(mesh.shape["ep"], 4, 2, 4), ("ep", *TP))
    return jax.shard_map(
        on_device,
        mesh=torus,
        in_specs=(
            P("ep", TP),
            P("ep", TP),
            P("ep", None),
            P("ep", None),
            P("ep", None, TP),
            P("ep", None, TP),
            P("ep", TP, None),
        ),
        out_specs=(
            P("ep", TP),
            P(("ep", *TP), None),
            P("ep", None, TP),
            P("ep", None, TP),
            P("ep", TP, None),
        ),
        check_vma=False,
    )
```

profile of v0, /device:TPU:1, one launch (start us, length us, event | category | flops | bytes accessed | tf_op | source)
XLA Modules:
  0.0 151.3 jit_solution(16822282197168283342)
XLA Ops:
  0.6 0.7 convert_bitcast_fusion.2
  1.3 0.7 convert_bitcast_fusion
  2.1 0.7 pad_maximum_fusion.table_ref
  2.7 0.4 shard_map.110
  3.1 0.0 copy-start.5
  3.1 27.5 %all_to_all.30 = bf16[24,16,128]{2,1,0:T(8,128)(2,1)S(1)} all-to-all(bf16[24,16,128]{2,1,0:T(8,128)(2,1)S(1)} %bitcast.33), channel_id=1, replica_groups=mesh['ep'=24,'yh'=4,'yl'=2,'x'=4] {'ep'}, dimensions={0} | all-to-all | bytes 196608 | tf_op jit(solution)/shard_map/all_to_all | solution.py:191
  30.6 0.0 copy-done.5
  30.6 0.1 shard_map.111
  30.7 19.0 %all_to_all.31 = bf16[4,128,384]{2,1,0:T(8,128)(2,1)S(1)} all-to-all(bf16[4,128,384]{2,1,0:T(8,128)(2,1)S(1)} %shard_map.111), channel_id=1, replica_groups=mesh['ep'=24,'yh'=4,'yl'=2,'x'=4] {'yh'}, dimensions={0} | all-to-all | bytes 786432 | tf_op jit(solution)/shard_map/all_to_all | solution.py:191
  49.8 0.5 broadcast_in_dim.15
  50.3 0.0 copy-start
  50.3 0.0 copy-start.1
  50.3 0.0 copy-start.2
  50.3 39.7 %all_to_all.32.rows_ref = bf16[8,4,128,384]{3,2,1,0:T(8,128)(2,1)S(1)} all-to-all(bf16[8,4,128,384]{3,2,1,0:T(8,128)(2,1)S(1)} %broadcast_in_dim.15), channel_id=1, replica_groups=mesh['ep'=24,'yh'=4,'yl'=2,'x'=4] {'yl','x'}, dimensions={0} | all-to-all | bytes 6291456 | tf_op jit(solution)/shard_map/all_to_all | solution.py:191
  90.0 0.0 copy-done
  90.0 0.0 copy-done.1
  90.0 0.0 copy-done.2
  90.0 2.5 %shard_map.112 = (bf16[8,264,384]{2,1,0:T(8,128)(2,1)S(1)}, bf16[528,384]{1,0:T(8,128)(2,1)S(1)}) custom-call(bf16[8,4,128,384]{3,2,1,0:T(8,128)(2,1)S(1)} %all_to_all.32.rows_ref, bf16[176,2048]{1,0:T(8,128)(2,1)S(1)} %bitcast.28, bf16[176,2048]{1,0:T(8,128)(2,1)S(1)} %bitcast.29, bf16[176,2048]{1,0:T(8,128)(2,1)S(1)} %bitcast.30), custom_call_target="tpu_custom_call" | custom-call | flops 1384120320 | bytes 5308416 | tf_op jit(solution)/shard_map/pallas_call | solution.py:24
  92.4 20.6 %all_to_all.33.in_ref = bf16[8,264,384]{2,1,0:T(8,128)(2,1)S(1)} all-to-all(bf16[8,264,384]{2,1,0:T(8,128)(2,1)S(1)} %get-tuple-element.15), channel_id=1, replica_groups=mesh['ep'=24,'yh'=4,'yl'=2,'x'=4] {'yl','x'}, dimensions={0} | all-to-all | bytes 3244032 | tf_op jit(solution)/shard_map/all_to_all | solution.py:191
  113.0 0.0 copy-start.4
  113.0 0.2 shard_map.113
  113.2 14.7 %all_to_all.34.in_ref = bf16[4,72,384]{2,1,0:T(8,128)(2,1)S(1)} all-to-all(bf16[4,72,384]{2,1,0:T(8,128)(2,1)S(1)} %shard_map.113), channel_id=1, replica_groups=mesh['ep'=24,'yh'=4,'yl'=2,'x'=4] {'yh'}, dimensions={0} | all-to-all | bytes 442368 | tf_op jit(solution)/shard_map/all_to_all | solution.py:191
  127.9 0.1 shard_map.114
  128.0 0.0 copy-start.3
  128.0 0.6 copy-done.3
  128.7 9.0 %all-to-all-start.5 = ((bf16[24,16,128]{2,1,0:T(8,128)(2,1)}), bf16[24,16,128]{2,1,0:T(8,128)(2,1)}, u32[]{:S(2)}, u32[]{:S(2)}) async-start(bf16[24,16,128]{2,1,0:T(8,128)(2,1)} %bitcast.31), calls=%async_computation.5 | async-start | bytes 196608 | tf_op jit(solution)/shard_map/all_to_all | solution.py:191
  137.7 2.7 %shard_map.116 = (bf16[176,2048]{1,0:T(8,128)(2,1)}, bf16[176,2048]{1,0:T(8,128)(2,1)}, bf16[176,2048]{1,0:T(8,128)(2,1)}) custom-call(bf16[528,384]{1,0:T(8,128)(2,1)S(1)} %get-tuple-element.19.parts_ref, bf16[8,4,128,384]{3,2,1,0:T(8,128)(2,1)S(1)} %all_to_all.32.rows_ref), custom_call_target="tpu_custom_call" | custom-call | flops 830472192 | bytes 3551232 | tf_op jit(solution)/shard_map/pallas_call | solution.py:24
  140.4 8.4 %all-to-all-done.5 = bf16[24,16,128]{2,1,0:T(8,128)(2,1)} async-done(((bf16[24,16,128]{2,1,0:T(8,128)(2,1)}), bf16[24,16,128]{2,1,0:T(8,128)(2,1)}, u32[]{:S(2)}, u32[]{:S(2)}) %all-to-all-start.5) | async-done | bytes 98336 | tf_op jit(solution)/shard_map/all_to_all | solution.py:191
  148.8 0.0 copy-done.4
  148.8 0.0 copy-start.6
  148.8 0.7 copy-done.6
  149.5 1.8 %shard_map.115 = (bf16[64,128]{1,0:T(8,128)(2,1)}, f32[2,4]{1,0:T(2,128)}) custom-call(s32[1]{0:T(128)} %bitcast.start_ref, bf16[384,128]{1,0:T(8,128)(2,1)} %bitcast.13.back_ref, s32[2,128]{1,0:T(2,128)S(1)} %copy-done.6, f32[2,128]{1,0:T(2,128)S(1)} %bitcast.35), custom_call_target="tpu_custom_call" | custom-call | bytes 100356 | tf_op jit(solution)/shard_map/pallas_call | solution.py:24
Async XLA Ops:
  3.1 27.5 %copy-start.5 = (s32[2,128]{1,0:T(2,128)}, s32[2,128]{1,0:T(2,128)S(1)}, u32[]{:S(2)}) copy-start(s32[2,128]{1,0:T(2,128)S(1)} %get-tuple-element.16.dest_ref) | copy-start | bytes 3076
  50.3 39.7 %copy-start = (bf16[1,2048,176]{1,2,0:T(8,128)(2,1)S(1)}, bf16[1,2048,176]{1,2,0:T(8,128)(2,1)}, u32[]{:S(2)}) copy-start(bf16[1,2048,176]{1,2,0:T(8,128)(2,1)} %param.11) | copy-start | bytes 2162692
  50.3 39.7 %copy-start.1 = (bf16[1,2048,176]{1,2,0:T(8,128)(2,1)S(1)}, bf16[1,2048,176]{1,2,0:T(8,128)(2,1)}, u32[]{:S(2)}) copy-start(bf16[1,2048,176]{1,2,0:T(8,128)(2,1)} %param.12) | copy-start | bytes 2162692
  50.3 39.7 %copy-start.2 = (bf16[1,176,2048]{2,1,0:T(8,128)(2,1)S(1)}, bf16[1,176,2048]{2,1,0:T(8,128)(2,1)}, u32[]{:S(2)}) copy-start(bf16[1,176,2048]{2,1,0:T(8,128)(2,1)} %param.13) | copy-start | bytes 2162692
  113.0 35.8 %copy-start.4 = (f32[128,2]{0,1:T(2,128)S(1)}, f32[128,2]{0,1:T(2,128)}, u32[]{:S(2)}) copy-start(f32[128,2]{0,1:T(2,128)} %param.10) | copy-start | bytes 3076
  128.0 0.6 copy-start.3
  128.7 20.1 %all-to-all-start.5 = ((bf16[24,16,128]{2,1,0:T(8,128)(2,1)}), bf16[24,16,128]{2,1,0:T(8,128)(2,1)}, u32[]{:S(2)}, u32[]{:S(2)}) async-start(bf16[24,16,128]{2,1,0:T(8,128)(2,1)} %bitcast.31), calls=%async_computation.5 | async-start | bytes 196608 | tf_op jit(solution)/shard_map/all_to_all | solution.py:191
  148.8 0.7 copy-start.6
where the time goes:
time: 152 us; the launch traced here: 151 us
  blocking collectives  121 us (80%)
  starting transfers between devices  9.02 us (6%)
  waiting for transfers between devices  8.39 us (6%)
  Pallas kernels  7.78 us (5%)
  other arithmetic  2.11 us (1%)
  local copies, waits for them, and re-layouts  1.8 us (1%)
    all_to_all x5, blocking collectives, exchange(): return lax.all_to_all(array, axis, split_axis=0, concat_axis=0, tiled=True)  121 us
    all_to_all x1, starting transfers between devices, exchange(): return lax.all_to_all(array, axis, split_axis=0, concat_axis=0, tiled=True)  9.02 us
    all_to_all x1, waiting for transfers between devices, exchange(): return lax.all_to_all(array, axis, split_axis=0, concat_axis=0, tiled=True)  8.39 us
    pallas_call x7, Pallas kernels, run(): pl.pallas_call(body, out_shape=[jax.ShapeDtypeStruct(s, d) for s, d in ou...  7.78 us
  transfers between devices with their start and end apart: 1, of which 1 were waited for; matrix products, arithmetic and copies ran while one was open for 0% of the time, Pallas kernels for 2%

commit v1 on v0

--- a/solution.py
+++ b/solution.py
@@ -201,9 +201,11 @@
     w_gate, w_up, w_down = gate_weight[0].T, up_weight[0].T, down_weight[0]
     hid, width = w_gate.shape
 
-    table = jnp.concatenate(
-        [a.T.astype(F32) for a in (tokens, out_grad, routes, gates)], axis=0
-    )
+    table = jnp.zeros((2 * feats + 2 * top_k, tok_dev), F32)
+    at = 0
+    for a in (tokens, out_grad, routes, gates):
+        table += jnp.pad(a.T, ((at, table.shape[0] - at - a.shape[1]), (0, 0))).astype(F32)
+        at += a.shape[1]
     sent, dest = call(
         functools.partial(place_body, n_ep=n_ep, cap=cap, top_k=top_k),
         [((rows, both), BF16), ((top_k, tok_dev), I32)],
@@ -221,7 +223,7 @@
     )(every, w_gate, w_up, w_down)
     swapped = exchange(chunks, NEAR)
     gate_grad, up_grad, down_grad = call(
-        weights_body, [((hid, width), BF16)] * 3, flops=6 * hid * width * rows, limit=20
+        weights_body, [((hid, width), BF16)] * 3, flops=6 * hid * width * rows, limit=60
     )(parts, every)
     (near,) = call(near_body, [((n_yh, feats + 8, rows), BF16)])(swapped)
     (packed,) = call(far_body, [((rows, both), BF16)])(exchange(near, "yh"))

time: 152 us -> 148 us (0.974)
  waiting for transfers between devices: 8.39 us -> 6.28 us
  Pallas kernels: 7.78 us -> 9.56 us
    all_to_all x1, waiting for transfers between devices: 8.39 us -> 6.28 us  [exchange(): return lax.all_to_all(array, axis, split_axis=0, concat_axis=0, tiled=True)]
    pallas_call x7, Pallas kernels: 7.78 us -> 9.56 us  [run(): pl.pallas_call(body, out_shape=[jax.ShapeDtypeStruct(s, d) for s, d in ou...]
  transfers between devices with their start and end apart: 1 -> 1, of which waited for: 1 -> 1; matrix products, arithmetic and copies ran while one was open for 0% -> 0% of each run, Pallas kernels for 2% -> 3%
where the time goes in v1:
time: 148 us
  blocking collectives  121 us (82%)
  Pallas kernels  9.56 us (6%)
  starting transfers between devices  8.4 us (6%)
  waiting for transfers between devices  6.28 us (4%)
    all_to_all x5, blocking collectives, exchange(): return lax.all_to_all(array, axis, split_axis=0, concat_axis=0, tiled=True)  121 us
    pallas_call x7, Pallas kernels, run(): pl.pallas_call(body, out_shape=[jax.ShapeDtypeStruct(s, d) for s, d in ou...  9.56 us
    all_to_all x1, starting transfers between devices, exchange(): return lax.all_to_all(array, axis, split_axis=0, concat_axis=0, tiled=True)  8.4 us
    all_to_all x1, waiting for transfers between devices, exchange(): return lax.all_to_all(array, axis, split_axis=0, concat_axis=0, tiled=True)  6.28 us
  transfers between devices with their start and end apart: 1, of which 1 were waited for; matrix products, arithmetic and copies ran while one was open for 0% of the time, Pallas kernels for 3%

profile of v1, /device:TPU:1, one launch (start us, length us, event | category | flops | bytes accessed | tf_op | source)
XLA Modules:
  0.0 147.7 jit_solution(16069183783315488271)
XLA Ops:
  0.6 0.8 pad_add_fusion.table_ref
  1.4 0.4 shard_map.110
  1.8 27.5 %all_to_all.30 = bf16[24,16,128]{2,1,0:T(8,128)(2,1)S(1)} all-to-all(bf16[24,16,128]{2,1,0:T(8,128)(2,1)S(1)} %bitcast.30), channel_id=1, replica_groups=mesh['ep'=24,'yh'=4,'yl'=2,'x'=4] {'ep'}, dimensions={0} | all-to-all | bytes 196608 | tf_op jit(solution)/shard_map/all_to_all | solution.py:191
  29.3 0.1 shard_map.111
  29.4 19.0 %all_to_all.31 = bf16[4,128,384]{2,1,0:T(8,128)(2,1)S(1)} all-to-all(bf16[4,128,384]{2,1,0:T(8,128)(2,1)S(1)} %shard_map.111), channel_id=1, replica_groups=mesh['ep'=24,'yh'=4,'yl'=2,'x'=4] {'yh'}, dimensions={0} | all-to-all | bytes 786432 | tf_op jit(solution)/shard_map/all_to_all | solution.py:191
  48.4 0.5 broadcast_in_dim.15
  48.9 0.0 copy-start.1
  48.9 0.0 copy-start.2
  48.9 0.0 copy-start.3
  49.0 39.7 %all_to_all.32.rows_ref = bf16[8,4,128,384]{3,2,1,0:T(8,128)(2,1)S(1)} all-to-all(bf16[8,4,128,384]{3,2,1,0:T(8,128)(2,1)S(1)} %broadcast_in_dim.15), channel_id=1, replica_groups=mesh['ep'=24,'yh'=4,'yl'=2,'x'=4] {'yl','x'}, dimensions={0} | all-to-all | bytes 6291456 | tf_op jit(solution)/shard_map/all_to_all | solution.py:191
  88.6 0.0 copy-start
  88.6 0.0 copy-done.1
  88.6 0.0 copy-done.2
  88.6 0.0 copy-done.3
  88.6 2.5 %shard_map.112 = (bf16[8,264,384]{2,1,0:T(8,128)(2,1)S(1)}, bf16[528,384]{1,0:T(8,128)(2,1)S(1)}) custom-call(bf16[8,4,128,384]{3,2,1,0:T(8,128)(2,1)S(1)} %all_to_all.32.rows_ref, bf16[176,2048]{1,0:T(8,128)(2,1)S(1)} %bitcast.25, bf16[176,2048]{1,0:T(8,128)(2,1)S(1)} %bitcast.26, bf16[176,2048]{1,0:T(8,128)(2,1)S(1)} %bitcast.27), custom_call_target="tpu_custom_call" | custom-call | flops 1384120320 | bytes 5308416 | tf_op jit(solution)/shard_map/pallas_call | solution.py:24
  91.1 0.0 copy-start.4
  91.1 20.6 %all_to_all.33.in_ref = bf16[8,264,384]{2,1,0:T(8,128)(2,1)S(1)} all-to-all(bf16[8,264,384]{2,1,0:T(8,128)(2,1)S(1)} %get-tuple-element.15), channel_id=1, replica_groups=mesh['ep'=24,'yh'=4,'yl'=2,'x'=4] {'yl','x'}, dimensions={0} | all-to-all | bytes 3244032 | tf_op jit(solution)/shard_map/all_to_all | solution.py:191
  111.7 0.0 copy-done
  111.7 0.0 copy-start.5
  111.7 0.2 shard_map.113
  111.9 14.7 %all_to_all.34.in_ref = bf16[4,72,384]{2,1,0:T(8,128)(2,1)S(1)} all-to-all(bf16[4,72,384]{2,1,0:T(8,128)(2,1)S(1)} %shard_map.113), channel_id=1, replica_groups=mesh['ep'=24,'yh'=4,'yl'=2,'x'=4] {'yh'}, dimensions={0} | all-to-all | bytes 442368 | tf_op jit(solution)/shard_map/all_to_all | solution.py:191
  126.6 0.8 shard_map.114
  127.4 0.0 copy-done.4
  127.4 8.4 %all-to-all-start.5 = ((bf16[24,16,128]{2,1,0:T(8,128)(2,1)}), bf16[24,16,128]{2,1,0:T(8,128)(2,1)S(1)}, u32[]{:S(2)}, u32[]{:S(2)}) async-start(bf16[24,16,128]{2,1,0:T(8,128)(2,1)} %bitcast.12), calls=%async_computation.5 | async-start | bytes 196608 | tf_op jit(solution)/shard_map/all_to_all | solution.py:191
  135.8 4.7 %shard_map.116 = (bf16[176,2048]{1,0:T(8,128)(2,1)}, bf16[176,2048]{1,0:T(8,128)(2,1)}, bf16[176,2048]{1,0:T(8,128)(2,1)}) custom-call(bf16[528,384]{1,0:T(8,128)(2,1)} %copy-done.4, bf16[8,4,128,384]{3,2,1,0:T(8,128)(2,1)} %copy-done), custom_call_target="tpu_custom_call" | custom-call | flops 830472192 | bytes 3551232 | tf_op jit(solution)/shard_map/pallas_call | solution.py:24
  140.5 6.3 %all-to-all-done.5 = bf16[24,16,128]{2,1,0:T(8,128)(2,1)S(1)} async-done(((bf16[24,16,128]{2,1,0:T(8,128)(2,1)}), bf16[24,16,128]{2,1,0:T(8,128)(2,1)S(1)}, u32[]{:S(2)}, u32[]{:S(2)}) %all-to-all-start.5) | async-done | bytes 98336 | tf_op jit(solution)/shard_map/all_to_all | solution.py:191
  146.8 0.0 copy-done.5
  146.8 0.9 shard_map.115
Async XLA Ops:
  48.9 39.7 %copy-start.1 = (bf16[1,2048,176]{1,2,0:T(8,128)(2,1)S(1)}, bf16[1,2048,176]{1,2,0:T(8,128)(2,1)}, u32[]{:S(2)}) copy-start(bf16[1,2048,176]{1,2,0:T(8,128)(2,1)} %param.11) | copy-start | bytes 2162692
  48.9 39.7 %copy-start.2 = (bf16[1,2048,176]{1,2,0:T(8,128)(2,1)S(1)}, bf16[1,2048,176]{1,2,0:T(8,128)(2,1)}, u32[]{:S(2)}) copy-start(bf16[1,2048,176]{1,2,0:T(8,128)(2,1)} %param.12) | copy-start | bytes 2162692
  48.9 39.7 %copy-start.3 = (bf16[1,176,2048]{2,1,0:T(8,128)(2,1)S(1)}, bf16[1,176,2048]{2,1,0:T(8,128)(2,1)}, u32[]{:S(2)}) copy-start(bf16[1,176,2048]{2,1,0:T(8,128)(2,1)} %param.13) | copy-start | bytes 2162692
  88.6 23.1 %copy-start = (bf16[8,4,128,384]{3,2,1,0:T(8,128)(2,1)}, bf16[8,4,128,384]{3,2,1,0:T(8,128)(2,1)S(1)}, u32[]{:S(2)}) copy-start(bf16[8,4,128,384]{3,2,1,0:T(8,128)(2,1)S(1)} %all_to_all.32.rows_ref) | copy-start | bytes 9437188
  91.1 36.3 %copy-start.4 = (bf16[528,384]{1,0:T(8,128)(2,1)}, bf16[528,384]{1,0:T(8,128)(2,1)S(1)}, u32[]{:S(2)}) copy-start(bf16[528,384]{1,0:T(8,128)(2,1)S(1)} %get-tuple-element.19.parts_ref) | copy-start | bytes 1216516
  111.7 35.1 %copy-start.5 = (f32[128,2]{0,1:T(2,128)S(1)}, f32[128,2]{0,1:T(2,128)}, u32[]{:S(2)}) copy-start(f32[128,2]{0,1:T(2,128)} %param.10) | copy-start | bytes 3076
  127.4 19.4 %all-to-all-start.5 = ((bf16[24,16,128]{2,1,0:T(8,128)(2,1)}), bf16[24,16,128]{2,1,0:T(8,128)(2,1)S(1)}, u32[]{:S(2)}, u32[]{:S(2)}) async-start(bf16[24,16,128]{2,1,0:T(8,128)(2,1)} %bitcast.12), calls=%async_computation.5 | async-start | bytes 196608 | tf_op jit(solution)/shard_map/all_to_all | solution.py:191

commit v2 on v1

--- a/solution.py
+++ b/solution.py
@@ -10,6 +10,7 @@
 
 TP = ("yh", "yl", "x")
 NEAR = ("yl", "x")
+FAR = ("ep", "yh")
 BF16 = jnp.bfloat16
 F32 = jnp.float32
 I32 = jnp.int32
@@ -73,13 +74,17 @@
         weight = weight + jnp.sum(jnp.where(at, gates[k : k + 1], 0.0), axis=1, keepdims=True)
     moved = dot(select.astype(BF16), table_ref[:both].astype(BF16), ((1,), (1,)))
     lane = iota(moved.shape, 1)
-    sent_ref[...] = jnp.where(lane < feats, moved, moved * weight).astype(BF16)
+    sent = jnp.where(lane < feats, moved, moved * weight).astype(BF16)
+    for k in range(sent_ref.shape[1]):
+        sent_ref[:, k] = sent.reshape(n_ep, cap, both)
 
 
 def turn_body(got_ref, out_ref):
-    turned = got_ref[...].astype(F32).T.astype(BF16)
-    for k in range(out_ref.shape[0]):
-        out_ref[k] = turned
+    n_ep, n_yh, cap, both = got_ref.shape
+    for yh in range(n_yh):
+        turned = got_ref[:, yh].reshape(n_ep * cap, both).astype(F32).T.astype(BF16)
+        for k in range(out_ref.shape[0]):
+            out_ref[k, yh] = turned
 
 
 def column(rows_ref, yh, yl, part):
@@ -138,41 +143,36 @@
             down_ref[:, cols] = dot(parts_ref[2 * hid :], c_t, ((1,), (1,))).astype(BF16)
 
 
-def near_body(in_ref, out_ref):
-    n, height, _ = in_ref.shape
-    n_y, tall, _ = out_ref.shape
-    feats = tall - 8
-    for y in range(n_y):
-        total = in_ref[0, y * feats : (y + 1) * feats].astype(F32)
+def sum_body(in_ref, out_ref):
+    n, height, rows = in_ref.shape
+    n_ep, n_yh, cap, both = out_ref.shape
+    feats = both // 2
+
+    def total(at):
+        whole = in_ref[0, at].astype(F32)
         for k in range(1, n):
-            total = total + in_ref[k, y * feats : (y + 1) * feats].astype(F32)
-        out_ref[y, :feats] = total.astype(BF16)
-    tail = in_ref[0, height - 8 :].astype(F32)
-    for k in range(1, n):
-        tail = tail + in_ref[k, height - 8 :].astype(F32)
-    tail = dot_rows(jnp.sum(tail, axis=0, keepdims=True)).astype(BF16)
-    for y in range(n_y):
-        out_ref[y, feats:] = tail
-
-
-def far_body(in_ref, out_ref):
-    n, tall, rows = in_ref.shape
-    total = in_ref[0].astype(F32)
-    for k in range(1, n):
-        total = total + in_ref[k].astype(F32)
-    feats = tall - 8
-    tail = dot_rows(jnp.sum(total[feats:], axis=0, keepdims=True))
-    rest = jnp.zeros((out_ref.shape[1] - tall, rows), F32)
-    whole = jnp.concatenate([total[:feats], tail, rest], axis=0)
-    out_ref[...] = whole.T.astype(BF16)
+            whole = whole + in_ref[k, at].astype(F32)
+        return whole
+
+    tail = total(slice(n_yh * feats, height))
+    tail = dot_rows(jnp.sum(tail, axis=0, keepdims=True))
+    rest = jnp.zeros((both - feats - 8, rows), F32)
+    for yh in range(n_yh):
+        block = total(slice(yh * feats, (yh + 1) * feats))
+        turned = jnp.concatenate([block, tail, rest], axis=0).T
+        out_ref[:, yh] = turned.astype(BF16).reshape(n_ep, cap, both)
 
 
 def final_body(start_ref, back_ref, dest_ref, gates_ref, tokens_ref, ratio_ref):
-    rows, lanes = back_ref.shape
+    n_ep, n_yh, cap, both = back_ref.shape
+    rows = n_ep * cap
     feats, toks = tokens_ref.shape
     top_k, share = ratio_ref.shape
-    back = back_ref[...]
-    dots = back[:, feats : feats + 1].astype(F32) + back[:, feats + 1 : feats + 2].astype(F32)
+    back = back_ref[:, 0].astype(F32)
+    for yh in range(1, n_yh):
+        back = back + back_ref[:, yh].astype(F32)
+    back = back.reshape(rows, both)
+    dots = back[:, feats : feats + 1] + back[:, feats + 1 : feats + 2]
     place = iota((rows, toks), 0)
     select = jnp.zeros((rows, toks), F32)
     start = start_ref[0]
@@ -183,7 +183,10 @@
         for j in range(share):
             here = iota((1, toks), 1) == start + j
             ratio_ref[k : k + 1, j : j + 1] = jnp.sum(jnp.where(here, mine, 0.0), axis=1, keepdims=True)
-    summed = dot(back, select.astype(BF16), ((0,), (0,)))
+    high = back.astype(BF16)
+    low = (back - high.astype(F32)).astype(BF16)
+    select = select.astype(BF16)
+    summed = dot(high, select, ((0,), (0,))) + dot(low, select, ((0,), (0,)))
     tokens_ref[...] = summed[:feats].astype(BF16)
 
 
@@ -208,12 +211,11 @@
         at += a.shape[1]
     sent, dest = call(
         functools.partial(place_body, n_ep=n_ep, cap=cap, top_k=top_k),
-        [((rows, both), BF16), ((top_k, tok_dev), I32)],
+        [((n_ep, n_yh, cap, both), BF16), ((top_k, tok_dev), I32)],
     )(table)
-    got = exchange(sent.reshape(n_ep, cap, both), "ep").reshape(rows, both)
-    (copies,) = call(turn_body, [((n_yh, both, rows), BF16)])(got)
-    some = exchange(copies, "yh")
-    every = exchange(jnp.broadcast_to(some[None], (n_near, *some.shape)), NEAR)
+    got = exchange(sent.reshape(n_ep * n_yh, cap, both), FAR).reshape(n_ep, n_yh, cap, both)
+    (copies,) = call(turn_body, [((n_near, n_yh, both, rows), BF16)])(got)
+    every = exchange(copies, NEAR)
 
     chunks, parts = call(
         expert_body,
@@ -225,9 +227,8 @@
     gate_grad, up_grad, down_grad = call(
         weights_body, [((hid, width), BF16)] * 3, flops=6 * hid * width * rows, limit=60
     )(parts, every)
-    (near,) = call(near_body, [((n_yh, feats + 8, rows), BF16)])(swapped)
-    (packed,) = call(far_body, [((rows, both), BF16)])(exchange(near, "yh"))
-    back = exchange(packed.reshape(n_ep, cap, both), "ep").reshape(rows, both)
+    (packed,) = call(sum_body, [((n_ep, n_yh, cap, both), BF16)])(swapped)
+    back = exchange(packed.reshape(n_ep * n_yh, cap, both), FAR).reshape(n_ep, n_yh, cap, both)
     share = tok_dev // (n_yh * n_near)
     start = (lax.axis_index(TP).astype(I32) * share).reshape(1)
     tokens_grad, ratio = call(

time: 148 us -> 150 us (1.014)
  waiting for transfers between devices: 6.28 us -> 18.4 us
  blocking collectives: 121 us -> 112 us
    all_to_all x1, waiting for transfers between devices: 6.28 us -> 18.4 us  [exchange(): return lax.all_to_all(array, axis, split_axis=0, concat_axis=0, tiled=True)]
    all_to_all x5 -> x3, blocking collectives: 121 us -> 112 us  [exchange(): return lax.all_to_all(array, axis, split_axis=0, concat_axis=0, tiled=True)]
    pallas_call x7 -> x6, Pallas kernels: 9.56 us -> 10 us  [run(): pl.pallas_call(body, out_shape=[jax.ShapeDtypeStruct(s, d) for s, d in ou...]
where the time goes in v2:
time: 150 us
  blocking collectives  112 us (75%)
  waiting for transfers between devices  18.4 us (12%)
  Pallas kernels  10 us (7%)
  starting transfers between devices  7.92 us (5%)
    all_to_all x3, blocking collectives, exchange(): return lax.all_to_all(array, axis, split_axis=0, concat_axis=0, tiled=True)  112 us
    all_to_all x1, waiting for transfers between devices, exchange(): return lax.all_to_all(array, axis, split_axis=0, concat_axis=0, tiled=True)  18.4 us
    pallas_call x6, Pallas kernels, run(): pl.pallas_call(body, out_shape=[jax.ShapeDtypeStruct(s, d) for s, d in ou...  10 us
    all_to_all x1, starting transfers between devices, exchange(): return lax.all_to_all(array, axis, split_axis=0, concat_axis=0, tiled=True)  7.92 us
  transfers between devices with their start and end apart: 1, of which 1 were waited for; matrix products, arithmetic and copies ran while one was open for 0% of the time, Pallas kernels for 3%

profile of v2, /device:TPU:1, one launch (start us, length us, event | category | flops | bytes accessed | tf_op | source)
XLA Modules:
  0.0 149.7 jit_solution(3049881116721268850)
XLA Ops:
  0.6 0.8 pad_add_fusion.table_ref
  1.4 0.4 shard_map.110
  1.8 45.7 %all_to_all.20 = bf16[96,16,128]{2,1,0:T(8,128)(2,1)S(1)} all-to-all(bf16[96,16,128]{2,1,0:T(8,128)(2,1)S(1)} %bitcast.30), channel_id=1, replica_groups=mesh['ep'=24,'yh'=4,'yl'=2,'x'=4] {'ep','yh'}, dimensions={0} | all-to-all | bytes 786432 | tf_op jit(solution)/shard_map/all_to_all | solution.py:194
  47.5 0.4 shard_map.111
  47.9 0.0 copy-start.1
  47.9 0.0 copy-start.2
  47.9 0.0 copy-start.3
  48.0 41.2 %all_to_all.21.rows_ref = bf16[8,4,128,384]{3,2,1,0:T(8,128)(2,1)S(1)} all-to-all(bf16[8,4,128,384]{3,2,1,0:T(8,128)(2,1)S(1)} %shard_map.111), channel_id=1, replica_groups=mesh['ep'=24,'yh'=4,'yl'=2,'x'=4] {'yl','x'}, dimensions={0} | all-to-all | bytes 6291456 | tf_op jit(solution)/shard_map/all_to_all | solution.py:194
  89.1 0.0 copy-start
  89.1 0.0 copy-done.1
  89.1 0.0 copy-done.2
  89.1 0.0 copy-done.3
  89.1 2.5 %shard_map.112 = (bf16[8,264,384]{2,1,0:T(8,128)(2,1)S(1)}, bf16[528,384]{1,0:T(8,128)(2,1)S(1)}) custom-call(bf16[8,4,128,384]{3,2,1,0:T(8,128)(2,1)S(1)} %all_to_all.21.rows_ref, bf16[176,2048]{1,0:T(8,128)(2,1)S(1)} %bitcast.27, bf16[176,2048]{1,0:T(8,128)(2,1)S(1)} %bitcast.28, bf16[176,2048]{1,0:T(8,128)(2,1)S(1)} %bitcast.29), custom_call_target="tpu_custom_call" | custom-call | flops 1384120320 | bytes 5308416 | tf_op jit(solution)/shard_map/pallas_call | solution.py:25
  91.6 0.0 copy-start.4
  91.6 25.0 %all_to_all.22.in_ref = bf16[8,264,384]{2,1,0:T(8,128)(2,1)S(1)} all-to-all(bf16[8,264,384]{2,1,0:T(8,128)(2,1)S(1)} %get-tuple-element.15), channel_id=1, replica_groups=mesh['ep'=24,'yh'=4,'yl'=2,'x'=4] {'yl','x'}, dimensions={0} | all-to-all | bytes 3244032 | tf_op jit(solution)/shard_map/all_to_all | solution.py:194
  116.6 0.0 copy-done
  116.6 0.0 copy-start.5
  116.6 1.1 shard_map.113
  117.7 0.0 copy-done.4
  117.7 7.9 %all-to-all-start.3 = ((bf16[96,16,128]{2,1,0:T(8,128)(2,1)}), bf16[96,16,128]{2,1,0:T(8,128)(2,1)S(1)}, u32[]{:S(2)}, u32[]{:S(2)}) async-start(bf16[96,16,128]{2,1,0:T(8,128)(2,1)} %bitcast.12), calls=%async_computation.3 | async-start | bytes 786432 | tf_op jit(solution)/shard_map/all_to_all | solution.py:194
  125.6 4.7 %shard_map.115 = (bf16[176,2048]{1,0:T(8,128)(2,1)}, bf16[176,2048]{1,0:T(8,128)(2,1)}, bf16[176,2048]{1,0:T(8,128)(2,1)}) custom-call(bf16[528,384]{1,0:T(8,128)(2,1)} %copy-done.4, bf16[8,4,128,384]{3,2,1,0:T(8,128)(2,1)} %copy-done), custom_call_target="tpu_custom_call" | custom-call | flops 830472192 | bytes 3551232 | tf_op jit(solution)/shard_map/pallas_call | solution.py:25
  130.3 18.4 %all-to-all-done.3 = bf16[96,16,128]{2,1,0:T(8,128)(2,1)S(1)} async-done(((bf16[96,16,128]{2,1,0:T(8,128)(2,1)}), bf16[96,16,128]{2,1,0:T(8,128)(2,1)S(1)}, u32[]{:S(2)}, u32[]{:S(2)}) %all-to-all-start.3) | async-done | bytes 393248 | tf_op jit(solution)/shard_map/all_to_all | solution.py:194
  148.7 0.0 copy-done.5
  148.7 1.0 shard_map.114
Async XLA Ops:
  47.9 41.2 %copy-start.1 = (bf16[1,2048,176]{1,2,0:T(8,128)(2,1)S(1)}, bf16[1,2048,176]{1,2,0:T(8,128)(2,1)}, u32[]{:S(2)}) copy-start(bf16[1,2048,176]{1,2,0:T(8,128)(2,1)} %param.11) | copy-start | bytes 2162692
  47.9 41.2 %copy-start.2 = (bf16[1,2048,176]{1,2,0:T(8,128)(2,1)S(1)}, bf16[1,2048,176]{1,2,0:T(8,128)(2,1)}, u32[]{:S(2)}) copy-start(bf16[1,2048,176]{1,2,0:T(8,128)(2,1)} %param.12) | copy-start | bytes 2162692
  47.9 41.2 %copy-start.3 = (bf16[1,176,2048]{2,1,0:T(8,128)(2,1)S(1)}, bf16[1,176,2048]{2,1,0:T(8,128)(2,1)}, u32[]{:S(2)}) copy-start(bf16[1,176,2048]{2,1,0:T(8,128)(2,1)} %param.13) | copy-start | bytes 2162692
  89.1 27.5 %copy-start = (bf16[8,4,128,384]{3,2,1,0:T(8,128)(2,1)}, bf16[8,4,128,384]{3,2,1,0:T(8,128)(2,1)S(1)}, u32[]{:S(2)}) copy-start(bf16[8,4,128,384]{3,2,1,0:T(8,128)(2,1)S(1)} %all_to_all.21.rows_ref) | copy-start | bytes 9437188
  91.6 26.1 %copy-start.4 = (bf16[528,384]{1,0:T(8,128)(2,1)}, bf16[528,384]{1,0:T(8,128)(2,1)S(1)}, u32[]{:S(2)}) copy-start(bf16[528,384]{1,0:T(8,128)(2,1)S(1)} %get-tuple-element.19.parts_ref) | copy-start | bytes 1216516
  116.6 32.1 %copy-start.5 = (f32[128,2]{0,1:T(2,128)S(1)}, f32[128,2]{0,1:T(2,128)}, u32[]{:S(2)}) copy-start(f32[128,2]{0,1:T(2,128)} %param.10) | copy-start | bytes 3076
  117.7 31.0 %all-to-all-start.3 = ((bf16[96,16,128]{2,1,0:T(8,128)(2,1)}), bf16[96,16,128]{2,1,0:T(8,128)(2,1)S(1)}, u32[]{:S(2)}, u32[]{:S(2)}) async-start(bf16[96,16,128]{2,1,0:T(8,128)(2,1)} %bitcast.12), calls=%async_computation.3 | async-start | bytes 786432 | tf_op jit(solution)/shard_map/all_to_all | solution.py:194

commit v3 on v1

--- a/solution.py
+++ b/solution.py
@@ -8,8 +8,8 @@
 from jax.sharding import Mesh
 from jax.sharding import PartitionSpec as P
 
-TP = ("yh", "yl", "x")
-NEAR = ("yl", "x")
+TP = ("yh", "yl", "xh", "xl")
+FAR = ("yh", "xh")
 BF16 = jnp.bfloat16
 F32 = jnp.float32
 I32 = jnp.int32
@@ -83,17 +83,18 @@
 
 
 def column(rows_ref, yh, yl, part):
-    _, _, both, _ = rows_ref.shape
+    feats = rows_ref.shape[2] // 2
+    at = slice(part * feats, (part + 1) * feats)
+    return jnp.concatenate(
+        [rows_ref[yl * 2 + xl, yh * 2 + xh, at] for xh in range(2) for xl in range(2)], axis=0
+    )
+
+
+def expert_body(rows_ref, wg_ref, wu_ref, wd_ref, out_ref, parts_ref):
+    n_near, n_far, both, _ = rows_ref.shape
+    n_yh = n_far // 2
     feats = both // 2
-    n_x = rows_ref.shape[0] // 2
-    at = slice(part * feats, (part + 1) * feats)
-    return jnp.concatenate([rows_ref[yl * n_x + x, yh, at] for x in range(n_x)], axis=0)
-
-
-def expert_body(rows_ref, wg_ref, wu_ref, wd_ref, out_ref, parts_ref):
-    n_near, n_yh, both, _ = rows_ref.shape
-    feats = both // 2
-    n_x = n_near // 2
+    n_x = 4
     hid = wg_ref.shape[0]
     order = [(yh, yl) for yh in range(n_yh) for yl in range(2)]
     x_t = jnp.concatenate([column(rows_ref, yh, yl, 0) for yh, yl in order], axis=0)
@@ -117,15 +118,15 @@
         w = jnp.concatenate([wg_ref[:, cols], wu_ref[:, cols]], axis=0)
         piece = dot(w, parts, ((0,), (0,))).astype(BF16)
         for x in range(n_x):
-            at = slice(yh * feats, (yh + 1) * feats)
-            out_ref[yl * n_x + x, at] = piece[x * feats : (x + 1) * feats]
+            at = (yh * 2 + x // 2) * feats
+            out_ref[yl * 2 + x % 2, at : at + feats] = piece[x * feats : (x + 1) * feats]
     for k in range(n_near):
-        out_ref[k, n_yh * feats :] = tail
+        out_ref[k, n_far * feats :] = tail
 
 
 def weights_body(parts_ref, rows_ref, gate_ref, up_ref, down_ref):
-    n_near, n_yh, both, _ = rows_ref.shape
-    wide = n_near // 2 * (both // 2)
+    n_yh = rows_ref.shape[1] // 2
+    wide = 4 * (rows_ref.shape[2] // 2)
     hid = gate_ref.shape[0]
     for yh in range(n_yh):
         for yl in range(2):
@@ -187,13 +188,28 @@
     tokens_ref[...] = summed[:feats].astype(BF16)
 
 
-def exchange(array, axis):
-    return lax.all_to_all(array, axis, split_axis=0, concat_axis=0, tiled=True)
+def exchange(array, axis, groups=None):
+    return lax.all_to_all(
+        array, axis, split_axis=0, concat_axis=0, tiled=True, axis_index_groups=groups
+    )
+
+
+def neighbours(n_ep, n_y, n_x):
+    groups = []
+    for ep in range(n_ep):
+        step = 2 * (ep % 2)
+        for y in range(1, n_y, 2):
+            for x in range(1, n_x, 2):
+                ys, xs = ((y - 1 + step) % n_y, y), ((x - 1 + step) % n_x, x)
+                groups.append([(ep * n_y + i) * n_x + j for i in ys for j in xs])
+    return groups
 
 
 def on_device(tokens, out_grad, routes, gates, gate_weight, up_weight, down_weight):
     tok_dev, top_k = routes.shape
-    n_ep, n_yh, n_near = lax.axis_size("ep"), lax.axis_size("yh"), lax.axis_size(NEAR)
+    n_ep, n_far, n_near = lax.axis_size("ep"), lax.axis_size(FAR), 4
+    whole = ("ep", *TP)
+    blocks = neighbours(n_ep, 2 * lax.axis_size("yh"), 2 * lax.axis_size("xh"))
     cap = (3 * tok_dev + n_ep - 1) // n_ep
     rows = n_ep * cap
     feats = tokens.shape[1]
@@ -211,24 +227,24 @@
         [((rows, both), BF16), ((top_k, tok_dev), I32)],
     )(table)
     got = exchange(sent.reshape(n_ep, cap, both), "ep").reshape(rows, both)
-    (copies,) = call(turn_body, [((n_yh, both, rows), BF16)])(got)
-    some = exchange(copies, "yh")
-    every = exchange(jnp.broadcast_to(some[None], (n_near, *some.shape)), NEAR)
+    (copies,) = call(turn_body, [((n_far, both, rows), BF16)])(got)
+    some = exchange(copies, FAR)
+    every = exchange(jnp.broadcast_to(some[None], (n_near, *some.shape)), whole, blocks)
 
     chunks, parts = call(
         expert_body,
-        [((n_near, n_yh * feats + 8, rows), BF16), ((3 * hid, rows), BF16)],
+        [((n_near, n_far * feats + 8, rows), BF16), ((3 * hid, rows), BF16)],
         flops=10 * hid * width * rows,
         limit=20,
     )(every, w_gate, w_up, w_down)
-    swapped = exchange(chunks, NEAR)
+    swapped = exchange(chunks, whole, blocks)
     gate_grad, up_grad, down_grad = call(
         weights_body, [((hid, width), BF16)] * 3, flops=6 * hid * width * rows, limit=60
     )(parts, every)
-    (near,) = call(near_body, [((n_yh, feats + 8, rows), BF16)])(swapped)
-    (packed,) = call(far_body, [((rows, both), BF16)])(exchange(near, "yh"))
+    (near,) = call(near_body, [((n_far, feats + 8, rows), BF16)])(swapped)
+    (packed,) = call(far_body, [((rows, both), BF16)])(exchange(near, FAR))
     back = exchange(packed.reshape(n_ep, cap, both), "ep").reshape(rows, both)
-    share = tok_dev // (n_yh * n_near)
+    share = tok_dev // (n_far * n_near)
     start = (lax.axis_index(TP).astype(I32) * share).reshape(1)
     tokens_grad, ratio = call(
         final_body, [((feats, tok_dev), BF16), ((top_k, share), F32)], n_scalars=1
@@ -243,7 +259,7 @@
 
 
 def solution(mesh):
-    torus = Mesh(mesh.devices.reshape(mesh.shape["ep"], 4, 2, 4), ("ep", *TP))
+    torus = Mesh(mesh.devices.reshape(mesh.shape["ep"], 4, 2, 2, 2), ("ep", *TP))
     return jax.shard_map(
         on_device,
         mesh=torus,

time: 148 us -> 143 us (0.966)
  starting transfers between devices: 8.4 us -> 3.81 us
    all_to_all x1, starting transfers between devices: 8.4 us -> 3.81 us  [exchange(): lax.all_to_all(array, axis, split_axis=0, concat_axis=0, tiled=True, axis...]
where the time goes in v3:
time: 143 us; the launch traced here: 142 us
  blocking collectives  121 us (85%)
  Pallas kernels  9.61 us (7%)
  waiting for transfers between devices  6.28 us (4%)
  starting transfers between devices  3.81 us (3%)
    all_to_all x5, blocking collectives, exchange(): lax.all_to_all(array, axis, split_axis=0, concat_axis=0, tiled=True, axis...  121 us
    pallas_call x7, Pallas kernels, run(): pl.pallas_call(body, out_shape=[jax.ShapeDtypeStruct(s, d) for s, d in ou...  9.61 us
    all_to_all x1, waiting for transfers between devices, exchange(): lax.all_to_all(array, axis, split_axis=0, concat_axis=0, tiled=True, axis...  6.28 us
    all_to_all x1, starting transfers between devices, exchange(): lax.all_to_all(array, axis, split_axis=0, concat_axis=0, tiled=True, axis...  3.81 us
  transfers between devices with their start and end apart: 1, of which 1 were waited for; matrix products, arithmetic and copies ran while one was open for 0% of the time, Pallas kernels for 3%

profile of v3, /device:TPU:1, one launch (start us, length us, event | category | flops | bytes accessed | tf_op | source)
XLA Modules:
  0.0 142.3 jit_solution(15474506536675044404)
XLA Ops:
  0.6 0.8 pad_add_fusion.table_ref
  1.4 0.4 shard_map.110
  1.8 27.5 %all_to_all.30 = bf16[24,16,128]{2,1,0:T(8,128)(2,1)S(1)} all-to-all(bf16[24,16,128]{2,1,0:T(8,128)(2,1)S(1)} %bitcast.30), channel_id=1, replica_groups=mesh['ep'=24,'yh'=4,'yl'=2,'xh'=2,'xl'=2] {'ep'}, dimensions={0} | all-to-all | bytes 196608 | tf_op jit(solution)/shard_map/all_to_all | solution.py:192
  29.3 0.1 shard_map.111
  29.4 32.0 %all_to_all.31 = bf16[8,128,384]{2,1,0:T(8,128)(2,1)S(1)} all-to-all(bf16[8,128,384]{2,1,0:T(8,128)(2,1)S(1)} %shard_map.111), channel_id=1, replica_groups=mesh['ep'=24,'yh'=4,'yl'=2,'xh'=2,'xl'=2] {'yh','xh'}, dimensions={0} | all-to-all | bytes 1572864 | tf_op jit(solution)/shard_map/all_to_all | solution.py:192
  61.4 0.5 broadcast_in_dim.15
  61.9 0.0 copy-start.1
  61.9 0.0 copy-start.2
  61.9 0.0 copy-start.3
  61.9 25.1 %all_to_all.32.rows_ref = bf16[4,8,128,384]{3,2,1,0:T(8,128)(2,1)S(1)} all-to-all(bf16[4,8,128,384]{3,2,1,0:T(8,128)(2,1)S(1)} %broadcast_in_dim.15), channel_id=1, replica_groups={{0,1,4,5},{2,3,6,7},{8,9,12,13},{10,11,14,15},{16,17,20,21},{18,19,22,2..., dimensions={0} | all-to-all | bytes 6291456 | tf_op jit(solution)/shard_map/all_to_all | solution.py:192
  87.0 0.0 copy-start
  87.0 0.0 copy-done.1
  87.0 0.0 copy-done.2
  87.0 0.0 copy-done.3
  87.0 2.4 %shard_map.112 = (bf16[4,520,384]{2,1,0:T(8,128)(2,1)S(1)}, bf16[528,384]{1,0:T(8,128)(2,1)S(1)}) custom-call(bf16[4,8,128,384]{3,2,1,0:T(8,128)(2,1)S(1)} %all_to_all.32.rows_ref, bf16[176,2048]{1,0:T(8,128)(2,1)S(1)} %bitcast.25, bf16[176,2048]{1,0:T(8,128)(2,1)S(1)} %bitcast.26, bf16[176,2048]{1,0:T(8,128)(2,1)S(1)} %bitcast.27), custom_call_target="tpu_custom_call" | custom-call | flops 1384120320 | bytes 5308416 | tf_op jit(solution)/shard_map/pallas_call | solution.py:24
  89.5 0.0 copy-start.4
  89.5 16.9 %all_to_all.33.in_ref = bf16[4,520,384]{2,1,0:T(8,128)(2,1)S(1)} all-to-all(bf16[4,520,384]{2,1,0:T(8,128)(2,1)S(1)} %get-tuple-element.15), channel_id=1, replica_groups={{0,1,4,5},{2,3,6,7},{8,9,12,13},{10,11,14,15},{16,17,20,21},{18,19,22,2..., dimensions={0} | all-to-all | bytes 3194880 | tf_op jit(solution)/shard_map/all_to_all | solution.py:192
  106.3 0.0 copy-done
  106.3 0.0 copy-start.5
  106.3 0.2 shard_map.113
  106.6 19.2 %all_to_all.34.in_ref = bf16[8,72,384]{2,1,0:T(8,128)(2,1)S(1)} all-to-all(bf16[8,72,384]{2,1,0:T(8,128)(2,1)S(1)} %shard_map.113), channel_id=1, replica_groups=mesh['ep'=24,'yh'=4,'yl'=2,'xh'=2,'xl'=2] {'yh','xh'}, dimensions={0} | all-to-all | bytes 884736 | tf_op jit(solution)/shard_map/all_to_all | solution.py:192
  125.8 0.8 shard_map.114
  126.6 0.0 copy-done.4
  126.6 3.8 %all-to-all-start.5 = ((bf16[24,16,128]{2,1,0:T(8,128)(2,1)}), bf16[24,16,128]{2,1,0:T(8,128)(2,1)S(1)}, u32[]{:S(2)}, u32[]{:S(2)}) async-start(bf16[24,16,128]{2,1,0:T(8,128)(2,1)} %bitcast.12), calls=%async_computation.5 | async-start | bytes 196608 | tf_op jit(solution)/shard_map/all_to_all | solution.py:192
  130.4 4.7 %shard_map.116 = (bf16[176,2048]{1,0:T(8,128)(2,1)}, bf16[176,2048]{1,0:T(8,128)(2,1)}, bf16[176,2048]{1,0:T(8,128)(2,1)}) custom-call(bf16[528,384]{1,0:T(8,128)(2,1)} %copy-done.4, bf16[4,8,128,384]{3,2,1,0:T(8,128)(2,1)} %copy-done), custom_call_target="tpu_custom_call" | custom-call | flops 830472192 | bytes 3551232 | tf_op jit(solution)/shard_map/pallas_call | solution.py:24
  135.1 6.3 %all-to-all-done.5 = bf16[24,16,128]{2,1,0:T(8,128)(2,1)S(1)} async-done(((bf16[24,16,128]{2,1,0:T(8,128)(2,1)}), bf16[24,16,128]{2,1,0:T(8,128)(2,1)S(1)}, u32[]{:S(2)}, u32[]{:S(2)}) %all-to-all-start.5) | async-done | bytes 98336 | tf_op jit(solution)/shard_map/all_to_all | solution.py:192
  141.4 0.0 copy-done.5
  141.4 0.9 shard_map.115
Async XLA Ops:
  61.9 25.1 %copy-start.1 = (bf16[1,2048,176]{1,2,0:T(8,128)(2,1)S(1)}, bf16[1,2048,176]{1,2,0:T(8,128)(2,1)}, u32[]{:S(2)}) copy-start(bf16[1,2048,176]{1,2,0:T(8,128)(2,1)} %param.11) | copy-start | bytes 2162692
  61.9 25.1 %copy-start.2 = (bf16[1,2048,176]{1,2,0:T(8,128)(2,1)S(1)}, bf16[1,2048,176]{1,2,0:T(8,128)(2,1)}, u32[]{:S(2)}) copy-start(bf16[1,2048,176]{1,2,0:T(8,128)(2,1)} %param.12) | copy-start | bytes 2162692
  61.9 25.1 %copy-start.3 = (bf16[1,176,2048]{2,1,0:T(8,128)(2,1)S(1)}, bf16[1,176,2048]{2,1,0:T(8,128)(2,1)}, u32[]{:S(2)}) copy-start(bf16[1,176,2048]{2,1,0:T(8,128)(2,1)} %param.13) | copy-start | bytes 2162692
  87.0 19.3 %copy-start = (bf16[4,8,128,384]{3,2,1,0:T(8,128)(2,1)}, bf16[4,8,128,384]{3,2,1,0:T(8,128)(2,1)S(1)}, u32[]{:S(2)}) copy-start(bf16[4,8,128,384]{3,2,1,0:T(8,128)(2,1)S(1)} %all_to_all.32.rows_ref) | copy-start | bytes 9437188
  89.5 37.1 %copy-start.4 = (bf16[528,384]{1,0:T(8,128)(2,1)}, bf16[528,384]{1,0:T(8,128)(2,1)S(1)}, u32[]{:S(2)}) copy-start(bf16[528,384]{1,0:T(8,128)(2,1)S(1)} %get-tuple-element.19.parts_ref) | copy-start | bytes 1216516
  106.3 35.1 %copy-start.5 = (f32[128,2]{0,1:T(2,128)S(1)}, f32[128,2]{0,1:T(2,128)}, u32[]{:S(2)}) copy-start(f32[128,2]{0,1:T(2,128)} %param.10) | copy-start | bytes 3076
  126.6 14.8 %all-to-all-start.5 = ((bf16[24,16,128]{2,1,0:T(8,128)(2,1)}), bf16[24,16,128]{2,1,0:T(8,128)(2,1)S(1)}, u32[]{:S(2)}, u32[]{:S(2)}) async-start(bf16[24,16,128]{2,1,0:T(8,128)(2,1)} %bitcast.12), calls=%async_computation.5 | async-start | bytes 196608 | tf_op jit(solution)/shard_map/all_to_all | solution.py:192

commit v4 on v3

--- a/solution.py
+++ b/solution.py
@@ -8,8 +8,10 @@
 from jax.sharding import Mesh
 from jax.sharding import PartitionSpec as P
 
-TP = ("yh", "yl", "xh", "xl")
-FAR = ("yh", "xh")
+TP = ("ya", "yb", "yl", "xh", "xl")
+FIRST = ("ep", "ya")
+SECOND = ("yb", "xh")
+FAR = ("ya", "yb", "xh")
 BF16 = jnp.bfloat16
 F32 = jnp.float32
 I32 = jnp.int32
@@ -73,25 +75,32 @@
         weight = weight + jnp.sum(jnp.where(at, gates[k : k + 1], 0.0), axis=1, keepdims=True)
     moved = dot(select.astype(BF16), table_ref[:both].astype(BF16), ((1,), (1,)))
     lane = iota(moved.shape, 1)
-    sent_ref[...] = jnp.where(lane < feats, moved, moved * weight).astype(BF16)
+    sent = jnp.where(lane < feats, moved, moved * weight).astype(BF16)
+    for k in range(sent_ref.shape[1]):
+        sent_ref[:, k] = sent.reshape(n_ep, cap, both)
 
 
 def turn_body(got_ref, out_ref):
-    turned = got_ref[...].astype(F32).T.astype(BF16)
-    for k in range(out_ref.shape[0]):
-        out_ref[k] = turned
+    n_ep, n_ya, cap, both = got_ref.shape
+    for ya in range(n_ya):
+        turned = got_ref[:, ya].reshape(n_ep * cap, both).astype(F32).T.astype(BF16)
+        for k in range(out_ref.shape[0]):
+            out_ref[k, ya] = turned
 
 
 def column(rows_ref, yh, yl, part):
-    feats = rows_ref.shape[2] // 2
+    feats = rows_ref.shape[3] // 2
+    n_yb = rows_ref.shape[1] // 2
+    ya, yb = yh // n_yb, yh % n_yb
     at = slice(part * feats, (part + 1) * feats)
     return jnp.concatenate(
-        [rows_ref[yl * 2 + xl, yh * 2 + xh, at] for xh in range(2) for xl in range(2)], axis=0
+        [rows_ref[yl * 2 + xl, yb * 2 + xh, ya, at] for xh in range(2) for xl in range(2)], axis=0
     )
 
 
 def expert_body(rows_ref, wg_ref, wu_ref, wd_ref, out_ref, parts_ref):
-    n_near, n_far, both, _ = rows_ref.shape
+    n_near, n_second, n_ya, both, _ = rows_ref.shape
+    n_far = n_second * n_ya
     n_yh = n_far // 2
     feats = both // 2
     n_x = 4
@@ -125,8 +134,8 @@
 
 
 def weights_body(parts_ref, rows_ref, gate_ref, up_ref, down_ref):
-    n_yh = rows_ref.shape[1] // 2
-    wide = 4 * (rows_ref.shape[2] // 2)
+    n_yh = rows_ref.shape[1] * rows_ref.shape[2] // 2
+    wide = 4 * (rows_ref.shape[3] // 2)
     hid = gate_ref.shape[0]
     for yh in range(n_yh):
         for yl in range(2):
@@ -205,11 +214,25 @@
     return groups
 
 
+def second_groups(n_ep, n_y, n_x):
+    groups = []
+    for ep in range(n_ep):
+        for a in range(0, n_y, 4):
+            for yl in range(2):
+                ys = ((a + 4 * (ep % 2)) % n_y + yl, a + 2 + yl)
+                for xl in range(2):
+                    xs = (xl, xl + 2)
+                    groups.append([(ep * n_y + i) * n_x + j for i in ys for j in xs])
+    return groups
+
+
 def on_device(tokens, out_grad, routes, gates, gate_weight, up_weight, down_weight):
     tok_dev, top_k = routes.shape
     n_ep, n_far, n_near = lax.axis_size("ep"), lax.axis_size(FAR), 4
     whole = ("ep", *TP)
-    blocks = neighbours(n_ep, 2 * lax.axis_size("yh"), 2 * lax.axis_size("xh"))
+    blocks = neighbours(n_ep, lax.axis_size(("ya", "yb", "yl")), 2 * lax.axis_size("xh"))
+    n_ya, n_second = lax.axis_size("ya"), lax.axis_size(SECOND)
+    pairs = second_groups(n_ep, lax.axis_size(("ya", "yb", "yl")), 2 * lax.axis_size("xh"))
     cap = (3 * tok_dev + n_ep - 1) // n_ep
     rows = n_ep * cap
     feats = tokens.shape[1]
@@ -224,11 +247,11 @@
         at += a.shape[1]
     sent, dest = call(
         functools.partial(place_body, n_ep=n_ep, cap=cap, top_k=top_k),
-        [((rows, both), BF16), ((top_k, tok_dev), I32)],
+        [((n_ep, n_ya, cap, both), BF16), ((top_k, tok_dev), I32)],
     )(table)
-    got = exchange(sent.reshape(n_ep, cap, both), "ep").reshape(rows, both)
-    (copies,) = call(turn_body, [((n_far, both, rows), BF16)])(got)
-    some = exchange(copies, FAR)
+    got = exchange(sent.reshape(n_ep * n_ya, cap, both), FIRST).reshape(n_ep, n_ya, cap, both)
+    (copies,) = call(turn_body, [((n_second, n_ya, both, rows), BF16)])(got)
+    some = exchange(copies, whole, pairs)
     every = exchange(jnp.broadcast_to(some[None], (n_near, *some.shape)), whole, blocks)
 
     chunks, parts = call(
@@ -259,7 +282,7 @@
 
 
 def solution(mesh):
-    torus = Mesh(mesh.devices.reshape(mesh.shape["ep"], 4, 2, 2, 2), ("ep", *TP))
+    torus = Mesh(mesh.devices.reshape(mesh.shape["ep"], 2, 2, 2, 2, 2), ("ep", *TP))
     return jax.shard_map(
         on_device,
         mesh=torus,

time: 143 us -> 141 us (0.986)
  blocking collectives: 121 us -> 119 us
where the time goes in v4:
time: 141 us
  blocking collectives  119 us (84%)
  Pallas kernels  9.61 us (7%)
  waiting for transfers between devices  6.24 us (4%)
  starting transfers between devices  3.65 us (3%)
    all_to_all x5, blocking collectives, exchange(): lax.all_to_all(array, axis, split_axis=0, concat_axis=0, tiled=True, axis...  119 us
    pallas_call x7, Pallas kernels, run(): pl.pallas_call(body, out_shape=[jax.ShapeDtypeStruct(s, d) for s, d in ou...  9.61 us
    all_to_all x1, waiting for transfers between devices, exchange(): lax.all_to_all(array, axis, split_axis=0, concat_axis=0, tiled=True, axis...  6.24 us
    all_to_all x1, starting transfers between devices, exchange(): lax.all_to_all(array, axis, split_axis=0, concat_axis=0, tiled=True, axis...  3.65 us
  transfers between devices with their start and end apart: 1, of which 1 were waited for; matrix products, arithmetic and copies ran while one was open for 0% of the time, Pallas kernels for 3%

profile of v4, /device:TPU:1, one launch (start us, length us, event | category | flops | bytes accessed | tf_op | source)
XLA Modules:
  0.0 140.7 jit_solution(7327174159115031132)
XLA Ops:
  0.6 0.8 pad_add_fusion.table_ref
  1.4 0.4 shard_map.110
  1.8 39.8 %all_to_all.30 = bf16[48,16,128]{2,1,0:T(8,128)(2,1)S(1)} all-to-all(bf16[48,16,128]{2,1,0:T(8,128)(2,1)S(1)} %bitcast.30), channel_id=1, replica_groups=mesh['ep'=24,'ya'=2,'yb'=2,'yl'=2,'xh'=2,'xl'=2] {'ep','ya'}, dimensions={0} | all-to-all | bytes 393216 | tf_op jit(solution)/shard_map/all_to_all | solution.py:201
  41.5 0.1 shard_map.111
  41.7 18.5 %all_to_all.31 = bf16[4,2,128,384]{3,2,1,0:T(8,128)(2,1)S(1)} all-to-all(bf16[4,2,128,384]{3,2,1,0:T(8,128)(2,1)S(1)} %shard_map.111), channel_id=1, replica_groups={{0,2,8,10},{1,3,9,11},{4,6,12,14},{5,7,13,15},{16,18,24,26},{17,19,25,2..., dimensions={0} | all-to-all | bytes 1572864 | tf_op jit(solution)/shard_map/all_to_all | solution.py:201
  60.2 0.5 broadcast_in_dim.15
  60.7 0.0 copy-start.1
  60.7 0.0 copy-start.2
  60.7 0.0 copy-start.3
  60.7 25.1 %all_to_all.32.rows_ref = bf16[4,4,2,128,384]{4,3,2,1,0:T(8,128)(2,1)S(1)} all-to-all(bf16[4,4,2,128,384]{4,3,2,1,0:T(8,128)(2,1)S(1)} %broadcast_in_dim.15), channel_id=1, replica_groups={{0,1,4,5},{2,3,6,7},{8,9,12,13},{10,11,14,15},{16,17,20,21},{18,19,22,2..., dimensions={0} | all-to-all | bytes 6291456 | tf_op jit(solution)/shard_map/all_to_all | solution.py:201
  85.8 0.0 copy-start
  85.8 0.0 copy-done.1
  85.8 0.0 copy-done.2
  85.8 0.0 copy-done.3
  85.8 2.5 %shard_map.112 = (bf16[4,520,384]{2,1,0:T(8,128)(2,1)S(1)}, bf16[528,384]{1,0:T(8,128)(2,1)S(1)}) custom-call(bf16[4,4,2,128,384]{4,3,2,1,0:T(8,128)(2,1)S(1)} %all_to_all.32.rows_ref, bf16[176,2048]{1,0:T(8,128)(2,1)S(1)} %bitcast.26, bf16[176,2048]{1,0:T(8,128)(2,1)S(1)} %bitcast.27, bf16[176,2048]{1,0:T(8,128)(2,1)S(1)} %bitcast.28), custom_call_target="tpu_custom_call" | custom-call | flops 1384120320 | bytes 5308416 | tf_op jit(solution)/shard_map/pallas_call | solution.py:26
  88.3 0.0 copy-start.4
  88.3 16.9 %all_to_all.33.in_ref = bf16[4,520,384]{2,1,0:T(8,128)(2,1)S(1)} all-to-all(bf16[4,520,384]{2,1,0:T(8,128)(2,1)S(1)} %get-tuple-element.15), channel_id=1, replica_groups={{0,1,4,5},{2,3,6,7},{8,9,12,13},{10,11,14,15},{16,17,20,21},{18,19,22,2..., dimensions={0} | all-to-all | bytes 3194880 | tf_op jit(solution)/shard_map/all_to_all | solution.py:201
  105.1 0.0 copy-done
  105.1 0.0 copy-start.5
  105.1 0.2 shard_map.113
  105.4 19.0 %all_to_all.34.in_ref = bf16[8,72,384]{2,1,0:T(8,128)(2,1)S(1)} all-to-all(bf16[8,72,384]{2,1,0:T(8,128)(2,1)S(1)} %shard_map.113), channel_id=1, replica_groups=mesh['ep'=24,'ya'=2,'yb'=2,'yl'=2,'xh'=2,'xl'=2] {'ya','yb','xh'}, dimensions={0} | all-to-all | bytes 884736 | tf_op jit(solution)/shard_map/all_to_all | solution.py:201
  124.4 0.8 shard_map.114
  125.2 0.0 copy-done.4
  125.2 3.7 %all-to-all-start.5 = ((bf16[24,16,128]{2,1,0:T(8,128)(2,1)}), bf16[24,16,128]{2,1,0:T(8,128)(2,1)S(1)}, u32[]{:S(2)}, u32[]{:S(2)}) async-start(bf16[24,16,128]{2,1,0:T(8,128)(2,1)} %bitcast.12), calls=%async_computation.5 | async-start | bytes 196608 | tf_op jit(solution)/shard_map/all_to_all | solution.py:201
  128.8 4.7 %shard_map.116 = (bf16[176,2048]{1,0:T(8,128)(2,1)}, bf16[176,2048]{1,0:T(8,128)(2,1)}, bf16[176,2048]{1,0:T(8,128)(2,1)}) custom-call(bf16[528,384]{1,0:T(8,128)(2,1)} %copy-done.4, bf16[4,4,2,128,384]{4,3,2,1,0:T(8,128)(2,1)} %copy-done), custom_call_target="tpu_custom_call" | custom-call | flops 830472192 | bytes 3551232 | tf_op jit(solution)/shard_map/pallas_call | solution.py:26
  133.6 6.2 %all-to-all-done.5 = bf16[24,16,128]{2,1,0:T(8,128)(2,1)S(1)} async-done(((bf16[24,16,128]{2,1,0:T(8,128)(2,1)}), bf16[24,16,128]{2,1,0:T(8,128)(2,1)S(1)}, u32[]{:S(2)}, u32[]{:S(2)}) %all-to-all-start.5) | async-done | bytes 98336 | tf_op jit(solution)/shard_map/all_to_all | solution.py:201
  139.8 0.0 copy-done.5
  139.8 0.9 shard_map.115
Async XLA Ops:
  60.7 25.1 %copy-start.1 = (bf16[1,2048,176]{1,2,0:T(8,128)(2,1)S(1)}, bf16[1,2048,176]{1,2,0:T(8,128)(2,1)}, u32[]{:S(2)}) copy-start(bf16[1,2048,176]{1,2,0:T(8,128)(2,1)} %param.11) | copy-start | bytes 2162692
  60.7 25.1 %copy-start.2 = (bf16[1,2048,176]{1,2,0:T(8,128)(2,1)S(1)}, bf16[1,2048,176]{1,2,0:T(8,128)(2,1)}, u32[]{:S(2)}) copy-start(bf16[1,2048,176]{1,2,0:T(8,128)(2,1)} %param.12) | copy-start | bytes 2162692
  60.7 25.1 %copy-start.3 = (bf16[1,176,2048]{2,1,0:T(8,128)(2,1)S(1)}, bf16[1,176,2048]{2,1,0:T(8,128)(2,1)}, u32[]{:S(2)}) copy-start(bf16[1,176,2048]{2,1,0:T(8,128)(2,1)} %param.13) | copy-start | bytes 2162692
  85.8 19.3 %copy-start = (bf16[4,4,2,128,384]{4,3,2,1,0:T(8,128)(2,1)}, bf16[4,4,2,128,384]{4,3,2,1,0:T(8,128)(2,1)S(1)}, u32[]{:S(2)}) copy-start(bf16[4,4,2,128,384]{4,3,2,1,0:T(8,128)(2,1)S(1)} %all_to_all.32.rows_ref) | copy-start | bytes 9437188
  88.3 36.9 %copy-start.4 = (bf16[528,384]{1,0:T(8,128)(2,1)}, bf16[528,384]{1,0:T(8,128)(2,1)S(1)}, u32[]{:S(2)}) copy-start(bf16[528,384]{1,0:T(8,128)(2,1)S(1)} %get-tuple-element.19.parts_ref) | copy-start | bytes 1216516
  105.1 34.7 %copy-start.5 = (f32[128,2]{0,1:T(2,128)S(1)}, f32[128,2]{0,1:T(2,128)}, u32[]{:S(2)}) copy-start(f32[128,2]{0,1:T(2,128)} %param.10) | copy-start | bytes 3076
  125.2 14.6 %all-to-all-start.5 = ((bf16[24,16,128]{2,1,0:T(8,128)(2,1)}), bf16[24,16,128]{2,1,0:T(8,128)(2,1)S(1)}, u32[]{:S(2)}, u32[]{:S(2)}) async-start(bf16[24,16,128]{2,1,0:T(8,128)(2,1)} %bitcast.12), calls=%async_computation.5 | async-start | bytes 196608 | tf_op jit(solution)/shard_map/all_to_all | solution.py:201

commit v5 on v4

--- a/solution.py
+++ b/solution.py
@@ -88,13 +88,22 @@
             out_ref[k, ya] = turned
 
 
+def around(i, j):
+    return 2 * i + (i ^ j)
+
+
+def circle(ys, xs, ep, n_y, n_x):
+    corners = ((0, 0), (0, 1), (1, 1), (1, 0))
+    return [(ep * n_y + ys[i]) * n_x + xs[j] for i, j in corners]
+
+
 def column(rows_ref, yh, yl, part):
     feats = rows_ref.shape[3] // 2
     n_yb = rows_ref.shape[1] // 2
     ya, yb = yh // n_yb, yh % n_yb
     at = slice(part * feats, (part + 1) * feats)
     return jnp.concatenate(
-        [rows_ref[yl * 2 + xl, yb * 2 + xh, ya, at] for xh in range(2) for xl in range(2)], axis=0
+        [rows_ref[around(yl, xl), around(yb, xh), ya, at] for xh in range(2) for xl in range(2)], axis=0
     )
 
 
@@ -128,7 +137,7 @@
         piece = dot(w, parts, ((0,), (0,))).astype(BF16)
         for x in range(n_x):
             at = (yh * 2 + x // 2) * feats
-            out_ref[yl * 2 + x % 2, at : at + feats] = piece[x * feats : (x + 1) * feats]
+            out_ref[around(yl, x % 2), at : at + feats] = piece[x * feats : (x + 1) * feats]
     for k in range(n_near):
         out_ref[k, n_far * feats :] = tail
 
@@ -210,7 +219,7 @@
         for y in range(1, n_y, 2):
             for x in range(1, n_x, 2):
                 ys, xs = ((y - 1 + step) % n_y, y), ((x - 1 + step) % n_x, x)
-                groups.append([(ep * n_y + i) * n_x + j for i in ys for j in xs])
+                groups.append(circle(ys, xs, ep, n_y, n_x))
     return groups
 
 
@@ -222,7 +231,7 @@
                 ys = ((a + 4 * (ep % 2)) % n_y + yl, a + 2 + yl)
                 for xl in range(2):
                     xs = (xl, xl + 2)
-                    groups.append([(ep * n_y + i) * n_x + j for i in ys for j in xs])
+                    groups.append(circle(ys, xs, ep, n_y, n_x))
     return groups
 
 

time: 141 us -> 142 us (level)
  blocking collectives: 119 us -> 121 us
where the time goes in v5:
time: 142 us
  blocking collectives  121 us (85%)
  Pallas kernels  9.61 us (7%)
  waiting for transfers between devices  5.73 us (4%)
  starting transfers between devices  3.65 us (3%)
    all_to_all x5, blocking collectives, exchange(): lax.all_to_all(array, axis, split_axis=0, concat_axis=0, tiled=True, axis...  121 us
    pallas_call x7, Pallas kernels, run(): pl.pallas_call(body, out_shape=[jax.ShapeDtypeStruct(s, d) for s, d in ou...  9.61 us
    all_to_all x1, waiting for transfers between devices, exchange(): lax.all_to_all(array, axis, split_axis=0, concat_axis=0, tiled=True, axis...  5.73 us
    all_to_all x1, starting transfers between devices, exchange(): lax.all_to_all(array, axis, split_axis=0, concat_axis=0, tiled=True, axis...  3.65 us
  transfers between devices with their start and end apart: 1, of which 1 were waited for; matrix products, arithmetic and copies ran while one was open for 0% of the time, Pallas kernels for 3%

profile of v5, /device:TPU:1, one launch (start us, length us, event | category | flops | bytes accessed | tf_op | source)
XLA Modules:
  0.0 141.6 jit_solution(6170841933848561556)
XLA Ops:
  0.6 0.8 pad_add_fusion.table_ref
  1.4 0.4 shard_map.110
  1.8 39.8 %all_to_all.30 = bf16[48,16,128]{2,1,0:T(8,128)(2,1)S(1)} all-to-all(bf16[48,16,128]{2,1,0:T(8,128)(2,1)S(1)} %bitcast.30), channel_id=1, replica_groups=mesh['ep'=24,'ya'=2,'yb'=2,'yl'=2,'xh'=2,'xl'=2] {'ep','ya'}, dimensions={0} | all-to-all | bytes 393216 | tf_op jit(solution)/shard_map/all_to_all | solution.py:210
  41.5 0.1 shard_map.111
  41.7 18.9 %all_to_all.31 = bf16[4,2,128,384]{3,2,1,0:T(8,128)(2,1)S(1)} all-to-all(bf16[4,2,128,384]{3,2,1,0:T(8,128)(2,1)S(1)} %shard_map.111), channel_id=1, replica_groups={{0,2,10,8},{1,3,11,9},{4,6,14,12},{5,7,15,13},{16,18,26,24},{17,19,27,2..., dimensions={0} | all-to-all | bytes 1572864 | tf_op jit(solution)/shard_map/all_to_all | solution.py:210
  60.5 0.5 broadcast_in_dim.15
  61.0 0.0 copy-start.1
  61.0 0.0 copy-start.2
  61.0 0.0 copy-start.3
  61.1 25.4 %all_to_all.32.rows_ref = bf16[4,4,2,128,384]{4,3,2,1,0:T(8,128)(2,1)S(1)} all-to-all(bf16[4,4,2,128,384]{4,3,2,1,0:T(8,128)(2,1)S(1)} %broadcast_in_dim.15), channel_id=1, replica_groups={{0,1,5,4},{2,3,7,6},{8,9,13,12},{10,11,15,14},{16,17,21,20},{18,19,23,2..., dimensions={0} | all-to-all | bytes 6291456 | tf_op jit(solution)/shard_map/all_to_all | solution.py:210
  86.5 0.0 copy-start
  86.5 0.0 copy-done.1
  86.5 0.0 copy-done.2
  86.5 0.0 copy-done.3
  86.5 2.4 %shard_map.112 = (bf16[4,520,384]{2,1,0:T(8,128)(2,1)S(1)}, bf16[528,384]{1,0:T(8,128)(2,1)S(1)}) custom-call(bf16[4,4,2,128,384]{4,3,2,1,0:T(8,128)(2,1)S(1)} %all_to_all.32.rows_ref, bf16[176,2048]{1,0:T(8,128)(2,1)S(1)} %bitcast.26, bf16[176,2048]{1,0:T(8,128)(2,1)S(1)} %bitcast.27, bf16[176,2048]{1,0:T(8,128)(2,1)S(1)} %bitcast.28), custom_call_target="tpu_custom_call" | custom-call | flops 1384120320 | bytes 5308416 | tf_op jit(solution)/shard_map/pallas_call | solution.py:26
  89.0 0.0 copy-start.4
  89.0 16.9 %all_to_all.33.in_ref = bf16[4,520,384]{2,1,0:T(8,128)(2,1)S(1)} all-to-all(bf16[4,520,384]{2,1,0:T(8,128)(2,1)S(1)} %get-tuple-element.15), channel_id=1, replica_groups={{0,1,5,4},{2,3,7,6},{8,9,13,12},{10,11,15,14},{16,17,21,20},{18,19,23,2..., dimensions={0} | all-to-all | bytes 3194880 | tf_op jit(solution)/shard_map/all_to_all | solution.py:210
  105.9 0.0 copy-done
  105.9 0.0 copy-start.5
  105.9 0.2 shard_map.113
  106.1 19.6 %all_to_all.34.in_ref = bf16[8,72,384]{2,1,0:T(8,128)(2,1)S(1)} all-to-all(bf16[8,72,384]{2,1,0:T(8,128)(2,1)S(1)} %shard_map.113), channel_id=1, replica_groups=mesh['ep'=24,'ya'=2,'yb'=2,'yl'=2,'xh'=2,'xl'=2] {'ya','yb','xh'}, dimensions={0} | all-to-all | bytes 884736 | tf_op jit(solution)/shard_map/all_to_all | solution.py:210
  125.8 0.8 shard_map.114
  126.6 0.0 copy-done.4
  126.6 3.7 %all-to-all-start.5 = ((bf16[24,16,128]{2,1,0:T(8,128)(2,1)}), bf16[24,16,128]{2,1,0:T(8,128)(2,1)S(1)}, u32[]{:S(2)}, u32[]{:S(2)}) async-start(bf16[24,16,128]{2,1,0:T(8,128)(2,1)} %bitcast.12), calls=%async_computation.5 | async-start | bytes 196608 | tf_op jit(solution)/shard_map/all_to_all | solution.py:210
  130.2 4.7 %shard_map.116 = (bf16[176,2048]{1,0:T(8,128)(2,1)}, bf16[176,2048]{1,0:T(8,128)(2,1)}, bf16[176,2048]{1,0:T(8,128)(2,1)}) custom-call(bf16[528,384]{1,0:T(8,128)(2,1)} %copy-done.4, bf16[4,4,2,128,384]{4,3,2,1,0:T(8,128)(2,1)} %copy-done), custom_call_target="tpu_custom_call" | custom-call | flops 830472192 | bytes 3551232 | tf_op jit(solution)/shard_map/pallas_call | solution.py:26
  135.0 5.7 %all-to-all-done.5 = bf16[24,16,128]{2,1,0:T(8,128)(2,1)S(1)} async-done(((bf16[24,16,128]{2,1,0:T(8,128)(2,1)}), bf16[24,16,128]{2,1,0:T(8,128)(2,1)S(1)}, u32[]{:S(2)}, u32[]{:S(2)}) %all-to-all-start.5) | async-done | bytes 98336 | tf_op jit(solution)/shard_map/all_to_all | solution.py:210
  140.7 0.0 copy-done.5
  140.7 0.9 shard_map.115
Async XLA Ops:
  61.0 25.5 %copy-start.1 = (bf16[1,2048,176]{1,2,0:T(8,128)(2,1)S(1)}, bf16[1,2048,176]{1,2,0:T(8,128)(2,1)}, u32[]{:S(2)}) copy-start(bf16[1,2048,176]{1,2,0:T(8,128)(2,1)} %param.11) | copy-start | bytes 2162692
  61.0 25.5 %copy-start.2 = (bf16[1,2048,176]{1,2,0:T(8,128)(2,1)S(1)}, bf16[1,2048,176]{1,2,0:T(8,128)(2,1)}, u32[]{:S(2)}) copy-start(bf16[1,2048,176]{1,2,0:T(8,128)(2,1)} %param.12) | copy-start | bytes 2162692
  61.0 25.5 %copy-start.3 = (bf16[1,176,2048]{2,1,0:T(8,128)(2,1)S(1)}, bf16[1,176,2048]{2,1,0:T(8,128)(2,1)}, u32[]{:S(2)}) copy-start(bf16[1,176,2048]{2,1,0:T(8,128)(2,1)} %param.13) | copy-start | bytes 2162692
  86.5 19.4 %copy-start = (bf16[4,4,2,128,384]{4,3,2,1,0:T(8,128)(2,1)}, bf16[4,4,2,128,384]{4,3,2,1,0:T(8,128)(2,1)S(1)}, u32[]{:S(2)}) copy-start(bf16[4,4,2,128,384]{4,3,2,1,0:T(8,128)(2,1)S(1)} %all_to_all.32.rows_ref) | copy-start | bytes 9437188
  89.0 37.6 %copy-start.4 = (bf16[528,384]{1,0:T(8,128)(2,1)}, bf16[528,384]{1,0:T(8,128)(2,1)S(1)}, u32[]{:S(2)}) copy-start(bf16[528,384]{1,0:T(8,128)(2,1)S(1)} %get-tuple-element.19.parts_ref) | copy-start | bytes 1216516
  105.9 34.8 %copy-start.5 = (f32[128,2]{0,1:T(2,128)S(1)}, f32[128,2]{0,1:T(2,128)}, u32[]{:S(2)}) copy-start(f32[128,2]{0,1:T(2,128)} %param.10) | copy-start | bytes 3076
  126.6 14.1 %all-to-all-start.5 = ((bf16[24,16,128]{2,1,0:T(8,128)(2,1)}), bf16[24,16,128]{2,1,0:T(8,128)(2,1)S(1)}, u32[]{:S(2)}, u32[]{:S(2)}) async-start(bf16[24,16,128]{2,1,0:T(8,128)(2,1)} %bitcast.12), calls=%async_computation.5 | async-start | bytes 196608 | tf_op jit(solution)/shard_map/all_to_all | solution.py:210
